TPU v7x, 512 devices: a whole 4x8x8 slice. The times are simulated.
512 devices in a mesh: ep: 32 (over z, x), tp: 16 (over y, core).
Axes of the slice: x: 4, y: 8, z: 8, core: 2. Of those that a mesh axis runs over, the one named last changes fastest.
Arguments:
- mixer_in: bfloat16 [4096, 2048], P('ep'), may hold values from -6 to 6
- mixer_gain: float32 [2048], replicated, may hold values from 0.1 to 1.9
- w_value: bfloat16 [2048, 1536], P(None, 'tp'), may hold values from -0.125 to 0.125
- w_gate: bfloat16 [2048, 1536], P(None, 'tp'), may hold values from -0.125 to 0.125
- w_taps: float32 [31, 1536], P(None, 'tp'), may hold values from -3 to 3
- channel_gain: float32 [1536], P('tp'), may hold values from 0.1 to 1.9
- w_output: bfloat16 [1536, 2048], P('tp'), may hold values from -0.15625 to 0.15625
- expert_in: bfloat16 [4096, 2048], P('ep'), may hold values from -6 to 6
- expert_gain: float32 [2048], replicated, may hold values from 0 to 8
- route_experts: int32 [4096, 4], P('ep'), may hold values from 0 to 31, all different within a row; in each aligned block of 128 rows (0 to 127, 128 to 255, ...) at most 32 rows name the same one
- route_scores: float32 [4096, 4], P('ep'), may hold values from -6 to 6
- expert_gate: bfloat16 [32, 2048, 2048], P('ep', None, 'tp'), may hold values from -0.125 to 0.125
- expert_up: bfloat16 [32, 2048, 2048], P('ep', None, 'tp'), may hold values from -0.125 to 0.125
- expert_down: bfloat16 [32, 2048, 2048], P('ep', 'tp'), may hold values from -0.125 to 0.125
Outputs:
- mixer_out: bfloat16 [4096, 2048], P('ep')
- expert_out: bfloat16 [4096, 2048], P('ep')
Inputs may be any that keep to these rules, and one draw needn't show every extreme that they name: `route_experts`: each row names 4 different experts. In each aligned block of 128 rows (the rows of one index of ep) no expert is named more than 32 times, a bound that some block reaches.
All inputs are finite; a program needn't handle non-finite values.
Results may differ from a plain program's by a relative error of at most 0.02.
Values may be sent and summed in bfloat16 or wider, within the bound.
No kernel may reach another device: no remote copies, remote signals or barrier semaphores. Data moves between devices by JAX's collectives and lax.ppermute only.
A program may use at most 64 MiB of HBM per device.

v0:
```python
import jax
import jax.numpy as jnp
from jax import lax
from jax.sharding import Mesh
from jax.sharding import PartitionSpec as P

CONV_CH = 1536
CONV_W = 31
TOP_K = 4
TP = ("tp_0", "tp_1")


epsilon = 1e-05
clamp_limit = 7.0
swish_slope = 1.702


def shifted(block, axis, distance):
    devices = range(lax.axis_size(axis))
    route = [(i - distance, i) for i in devices if i - distance in devices]
    return lax.ppermute(block, axis, route)


def sent_to_all(x, axis):
    copies = jnp.broadcast_to(x, (lax.axis_size(axis), *x.shape))
    return lax.all_to_all(copies, axis, split_axis=0, concat_axis=0, tiled=True)


def over_copies(x, axis):
    everything = sent_to_all(x, axis)
    return jnp.sum(everything, axis=0)


def packed_total(arrays, axis):
    line, at, done = (jnp.concatenate([a.reshape(-1) for a in arrays]), 0, [])
    subtotal = over_copies(line, axis)
    for a in arrays:
        done.append(subtotal[at : at + a.size].reshape(a.shape))
        at += a.size
    return tuple(done)


def by_axis(x, axes):
    for axis in axes:
        x = lax.psum(x, axis)
    return x


def row_norm(inputs, gains):
    widened = inputs.astype(jnp.float32)
    row_mean = jnp.mean(widened, axis=-1, keepdims=True)
    row_var = jnp.mean(jnp.square(widened - row_mean), axis=-1, keepdims=True)
    return (widened - row_mean) * lax.rsqrt(row_var + epsilon) * gains


def local(
    mixer_in,
    mixer_gain,
    w_value,
    w_gate,
    w_taps,
    channel_gain,
    w_output,
    expert_in,
    expert_gain,
    route_experts,
    route_scores,
    expert_gate,
    expert_up,
    expert_down,
):
    normed = row_norm(mixer_in, mixer_gain).astype(jnp.bfloat16)
    values = jnp.dot(normed, w_value, preferred_element_type=jnp.float32)
    gate_pre = jnp.dot(normed, w_gate, preferred_element_type=jnp.float32)
    gated_values = (values * jax.nn.sigmoid(gate_pre)).astype(jnp.bfloat16)
    mixer_rows = gated_values.shape[0]
    reach_rows = CONV_W - 1
    earlier = shifted(gated_values[mixer_rows - reach_rows :], "ep", 1)
    extended = jnp.concatenate([earlier, gated_values], axis=0)
    conv_out = jnp.zeros(gated_values.shape, jnp.float32)
    for offset in range(CONV_W):
        conv_out = (
            conv_out + extended[offset : offset + mixer_rows].astype(jnp.float32) * w_taps[offset]
        )
    channel_sums = packed_total(
        (
            jnp.sum(conv_out, axis=1, keepdims=True),
            jnp.sum(conv_out * conv_out, axis=1, keepdims=True),
        ),
        TP,
    )
    row_mean = channel_sums[0] / CONV_CH
    row_var = channel_sums[1] / CONV_CH - row_mean * row_mean
    activated = jax.nn.silu(
        (conv_out - row_mean) * lax.rsqrt(row_var + epsilon) * channel_gain
    ).astype(jnp.bfloat16)
    mixer_out = (
        by_axis(
            jnp.dot(activated, w_output, preferred_element_type=jnp.float32).astype(jnp.bfloat16),
            TP,
        )
        .astype(jnp.float32)
        .astype(jnp.bfloat16)
    )
    rows_b = expert_in.shape[0]
    width = expert_in.shape[1]
    experts = lax.axis_size("ep")
    capacity = 2 * rows_b * TOP_K // experts
    slot_share = capacity // lax.axis_size(TP)
    column = lax.axis_index(TP)
    normed_b = row_norm(expert_in, expert_gain).astype(jnp.bfloat16)
    raised = jnp.exp(route_scores)
    route_weights = raised / jnp.sum(raised, axis=1, keepdims=True)
    flat_ids = route_experts.reshape(-1)
    onehot = (flat_ids[:, None] == jnp.arange(experts, dtype=jnp.int32)[None, :]).astype(jnp.int32)
    slot_index = jnp.sum((jnp.cumsum(onehot, axis=0) - onehot) * onehot, axis=1)
    owner_row = jnp.arange(rows_b * TOP_K, dtype=jnp.int32) // TOP_K
    slot_table = (
        jnp.full((capacity * experts,), rows_b, jnp.int32)
        .at[slot_index * experts + flat_ids]
        .set(owner_row)
    )
    padded = jnp.concatenate([normed_b, jnp.zeros((1, width), jnp.bfloat16)], axis=0)
    gate_w = expert_gate[0]
    up_w = expert_up[0]
    down_w = expert_down[0]
    own_table = lax.dynamic_slice_in_dim(
        slot_table, column * slot_share * experts, slot_share * experts
    )
    sending = jnp.take(padded, own_table, axis=0).reshape(slot_share, experts, width)
    arrived = lax.all_to_all(sending, "ep", split_axis=1, concat_axis=1, tiled=True)
    block_rows = lax.all_gather(arrived, TP, axis=0, tiled=True)
    flat_rows = block_rows.reshape(block_rows.shape[0] * block_rows.shape[1], block_rows.shape[2])
    gate_e = jnp.minimum(
        jnp.dot(flat_rows, gate_w, preferred_element_type=jnp.float32), clamp_limit
    )
    up_e = jnp.clip(
        jnp.dot(flat_rows, up_w, preferred_element_type=jnp.float32), -clamp_limit, clamp_limit
    )
    hidden = (
        ((up_e + 1.0) * gate_e * jax.nn.sigmoid(swish_slope * gate_e))
        .astype(jnp.bfloat16)
        .reshape(block_rows.shape[0], block_rows.shape[1], gate_w.shape[1])
        .reshape(capacity * experts, gate_w.shape[1])
    )
    summed = lax.psum_scatter(
        jnp.dot(hidden, down_w, preferred_element_type=jnp.float32).astype(jnp.bfloat16),
        TP,
        scatter_dimension=0,
        tiled=True,
    )
    returned = lax.all_to_all(
        summed.reshape(slot_share, experts, width), "ep", split_axis=1, concat_axis=1, tiled=True
    )
    every_slot = lax.all_gather(returned, TP, axis=0, tiled=True).reshape(capacity * experts, width)
    picked = jnp.take(every_slot, slot_index * experts + flat_ids, axis=0)
    picked = picked.reshape(rows_b, TOP_K, width).astype(jnp.float32)
    expert_out = jnp.sum(picked * route_weights[:, :, None], axis=1).astype(jnp.bfloat16)
    return (mixer_out, expert_out)


def solution(mesh):
    split = Mesh(mesh.devices.reshape(mesh.shape["ep"], 8, 2), ("ep", "tp_0", "tp_1"))
    in_specs = (
        P("ep", None),
        P(),
        P(None, TP),
        P(None, TP),
        P(None, TP),
        P(TP),
        P(TP, None),
        P("ep", None),
        P(),
        P("ep", None),
        P("ep", None),
        P("ep", None, TP),
        P("ep", None, TP),
        P("ep", TP, None),
    )
    out_specs = (P("ep", None), P("ep", None))
    return jax.shard_map(local, mesh=split, in_specs=in_specs, out_specs=out_specs, check_vma=False)
```

profile of v0, /device:TPU:1, one launch (start us, length us, event | category | flops | bytes accessed | tf_op | source)
XLA Modules:
  0.0 251.4 jit_solution(10205323536202366580)
XLA Ops:
  8.1 0.9 copy.59
  9.0 0.1 eq.29
  9.1 0.1 eq.25
  9.2 0.1 reshape.133
  9.3 1.2 reduce-window.6
  10.5 0.2 slice_reduce_fusion
  10.7 0.1 fusion.34
  10.9 2.4 scatter_custom_fusion
  13.3 0.1 compare_and_fusion
  13.4 1.2 convert_reduce_fusion
  14.6 1.3 fusion.13
  16.0 0.1 broadcast_in_dim.45
  16.1 0.1 copy.65
  16.2 1.4 fusion.15
  17.6 0.7 gather_fusion
  18.4 0.3 broadcast_select_fusion
  18.7 24.8 %all_to_all.16 = bf16[2,32,2048]{2,0,1:T(2,128)(2,1)S(1)} all-to-all(bf16[2,32,2048]{2,0,1:T(2,128)(2,1)S(1)} %broadcast_select_fusion), channel_id=1, replica_groups=mesh['ep'=32,'tp_0'=8,'tp_1'=2] {'ep'}, dimensions={1} | all-to-all | bytes 524288 | tf_op jit(solution)/shard_map/all_to_all | solution.py:131
  43.6 0.8 copy.67
  44.4 42.1 %all-gather.3.cloned.1.call-done = bf16[32,32,2048]{2,1,0:T(8,128)(2,1)} async-done(((bf16[2,32,2048]{2,1,0:T(8,128)(2,1)}), bf16[32,32,2048]{2,1,0:T(8,128)(2,1)}) %all-gather.3.cloned.1.call-update) | async-done | bytes 4194320 | tf_op jit(solution)/shard_map/all_gather | solution.py:132
  86.5 3.4 %convolution_minimum_fusion = f32[1024,128]{1,0:T(8,128)S(1)} fusion(bf16[1024,2048]{1,0:T(8,128)(2,1)} %bitcast.103, bf16[1,2048,128]{2,1,0:T(8,128)(2,1)S(1)} %copy-done.8), kind=kOutput, calls=%fused_computation.14 | convolution fusion | flops 537001984 | bytes 5242880 | tf_op jit(solution)/shard_map/dot_general | solution.py:135
  90.0 8.5 %convolution_convert_fusion = bf16[1024,2048]{1,0:T(8,128)(2,1)} fusion(f32[1024,128]{1,0:T(8,128)S(1)} %convolution_minimum_fusion, bf16[1024,2048]{1,0:T(8,128)(2,1)} %bitcast.104, bf16[1,128,2048]{2,1,0:T(8,128)(2,1)S(1)} %copy-done, bf16[1,2048,128]{2,1,0:T(8,128)(2,1)S(1)} %copy-done.2), kind=kOutput, calls=%fused_computation.4 | convolution fusion | flops 1077018624 | bytes 9961472 | tf_op jit(solution)/shard_map/dot_general | solution.py:147
  98.6 0.0 all-reduce.4.cloned.1.call-start
  98.6 0.9 copy-done.1
  99.5 0.2 convert_reduce_fusion.1
  99.7 0.3 fusion.16
  100.0 0.4 fusion.80
  100.4 0.4 fusion.12
  100.8 0.1 slice.268
  100.9 3.1 %collective-permute-start = (bf16[30,96]{0,1:T(8,128)(2,1)S(1)}, bf16[30,96]{0,1:T(8,128)(2,1)S(1)}, u32[]{:S(2)}, u32[]{:S(2)}) collective-permute-start(bf16[30,96]{0,1:T(8,128)(2,1)S(1)} %slice.268), channel_id=1, source_target_pairs={{0,16},{16,32},{32,48},{48,64},{64,80},{80,96},{96,112},{112,128},... | collective-permute-start | bytes 17288 | tf_op jit(solution)/shard_map/ppermute | solution.py:21
  104.1 0.9 collective-permute-done
  104.9 0.9 fusion.82
  105.8 12.5 %all_to_all.17 = f32[16,1,256]{2,1,0:T(1,128)S(1)} all-to-all(f32[16,1,256]{2,1,0:T(1,128)S(1)} %broadcast_in_dim.42), channel_id=1, replica_groups=mesh['ep'=32,'tp_0'=8,'tp_1'=2] {'tp_0','tp_1'}, dimensions={0} | all-to-all | bytes 32768 | tf_op jit(solution)/shard_map/all_to_all | solution.py:26
  118.4 1.2 convolution_convert_fusion.1
  119.6 42.9 %reduce-scatter.2.cloned.1.call-done = bf16[64,2048]{1,0:T(8,128)(2,1)} async-done(((bf16[1024,2048]{1,0:T(8,128)(2,1)}), bf16[64,2048]{1,0:T(8,128)(2,1)}) %reduce-scatter.2.cloned.1.call-update) | async-done | bytes 262160 | tf_op jit(solution)/shard_map/reduce_scatter | solution.py:146
  162.5 1.2 copy.68
  163.8 18.9 %all_to_all.18 = bf16[2,32,2048]{2,0,1:T(2,128)(2,1)S(1)} all-to-all(bf16[2,32,2048]{2,0,1:T(2,128)(2,1)S(1)} %copy.68), channel_id=1, replica_groups=mesh['ep'=32,'tp_0'=8,'tp_1'=2] {'ep'}, dimensions={1} | all-to-all | bytes 524288 | tf_op jit(solution)/shard_map/all_to_all | solution.py:152
  182.7 0.8 copy.69
  183.5 0.2 all-reduce.6.cloned.1.call-start
  183.7 0.1 mul.529
  183.8 0.1 copy.62
  183.9 0.1 copy.63
  184.1 0.1 copy.70
  184.2 9.5 %all-reduce.4.cloned.1.call-done = bf16[128,2048]{1,0:T(8,128)(2,1)} async-done(((bf16[128,2048]{1,0:T(8,128)(2,1)}), bf16[128,2048]{1,0:T(8,128)(2,1)}) %all-reduce.4.cloned.1.call-update) | async-done | bytes 524304 | tf_op jit(solution)/shard_map/psum | solution.py:45
  193.8 32.8 %all-gather.5.cloned.1.call-done = bf16[32,32,2048]{2,1,0:T(8,128)(2,1)} async-done(((bf16[2,32,2048]{2,1,0:T(8,128)(2,1)}), bf16[32,32,2048]{2,1,0:T(8,128)(2,1)}) %all-gather.5.cloned.1.call-update) | async-done | bytes 4194320 | tf_op jit(solution)/shard_map/all_gather | solution.py:155
  226.6 7.1 %gather_fusion.1 = bf16[512,2048]{1,0:T(8,128)(2,1)S(1)} fusion(bf16[1024,2048]{1,0:T(8,128)(2,1)} %bitcast.102, s32[1024]{0:T(1024)S(1)} %pad_clamp_fusion), kind=kCustom, calls=%fused_computation.1 | custom fusion | bytes 4196352 | tf_op jit(solution)/shard_map/jit(_take)/gather | solution.py:156
  233.7 2.2 gather.15
  236.0 6.4 %multiply_reduce_fusion = bf16[128,2048]{1,0:T(8,128)(2,1)} fusion(f32[128,4]{1,0:T(8,128)S(1)} %copy.70, bf16[128,4,2048]{2,1,0:T(4,128)(2,1)} %gather.15, pred[128,4]{1,0:T(8,128)(4,1)S(1)} %copy.63), kind=kLoop, calls=%fused_computation.3 | loop fusion | flops 3932160 | bytes 2624000 | tf_op jit(solution)/shard_map/reduce_sum | solution.py:158
  242.4 1.9 copy.79
  (54 shorter events, 0.6 us)
Async XLA Ops:
  8.0 82.0 %copy-start = (bf16[1,128,2048]{2,1,0:T(8,128)(2,1)S(1)}, bf16[1,128,2048]{2,1,0:T(8,128)(2,1)}, u32[]{:S(2)}) copy-start(bf16[1,128,2048]{2,1,0:T(8,128)(2,1)} %param.27) | copy-start | bytes 1572868
  8.0 78.5 %copy-start.8 = (bf16[1,2048,128]{2,1,0:T(8,128)(2,1)S(1)}, bf16[1,2048,128]{2,1,0:T(8,128)(2,1)}, u32[]{:S(2)}) copy-start(bf16[1,2048,128]{2,1,0:T(8,128)(2,1)} %param.25) | copy-start | bytes 1572868
  8.0 78.5 %all-gather.3.cloned.1.call-start = ((), (), s32[]{:S(2)}) async-start(), calls=%async_computation.6 | async-start | bytes 4456448 | tf_op jit(solution)/shard_map/all_gather | solution.py:132
  18.4 71.6 %copy-start.2 = (bf16[1,2048,128]{2,1,0:T(8,128)(2,1)S(1)}, bf16[1,2048,128]{2,1,0:T(8,128)(2,1)}, u32[]{:S(2)}) copy-start(bf16[1,2048,128]{2,1,0:T(8,128)(2,1)} %param.26) | copy-start | bytes 1572868
  44.4 118.2 %reduce-scatter.2.cloned.1.call-start = ((), (), s32[]{:S(2)}) async-start(), calls=%async_computation.7 | async-start | bytes 4456448 | tf_op jit(solution)/shard_map/reduce_scatter | solution.py:146
  98.5 1.0 copy-start.1
  98.5 1.5 copy-start.9
  98.5 1.5 copy-start.11
  98.5 1.9 copy-start.10
  98.5 5.5 %copy-start.4 = (f32[31,96]{1,0:T(8,128)S(1)}, f32[31,96]{1,0:T(8,128)}, u32[]{:S(2)}) copy-start(f32[31,96]{1,0:T(8,128)} %param.18) | copy-start | bytes 35716
  98.5 19.9 %copy-start.3 = (bf16[96,2048]{1,0:T(8,128)(2,1)S(1)}, bf16[96,2048]{1,0:T(8,128)(2,1)}, u32[]{:S(2)}) copy-start(bf16[96,2048]{1,0:T(8,128)(2,1)} %param.20) | copy-start | bytes 1179652
  98.5 19.8 %copy-start.7 = (f32[96]{0:T(128)S(1)}, f32[96]{0:T(128)}, u32[]{:S(2)}) copy-start(f32[96]{0:T(128)} %param.19) | copy-start | bytes 1156
  98.5 85.3 %copy-start.5 = (s32[128,4]{0,1:T(4,128)S(1)}, s32[128,4]{0,1:T(4,128)}, u32[]{:S(2)}) copy-start(s32[128,4]{0,1:T(4,128)} %param.23) | copy-start | bytes 6148
  98.6 85.5 %copy-start.6 = (f32[128,4]{0,1:T(4,128)S(1)}, f32[128,4]{0,1:T(4,128)}, u32[]{:S(2)}) copy-start(f32[128,4]{0,1:T(4,128)} %param.24) | copy-start | bytes 6148
  98.6 95.1 %all-reduce.4.cloned.1.call-start = ((), (), s32[]{:S(2)}) async-start(), calls=%async_computation.4 | async-start | bytes 1048576 | tf_op jit(solution)/shard_map/psum | solution.py:45
  100.9 4.0 %collective-permute-start = (bf16[30,96]{0,1:T(8,128)(2,1)S(1)}, bf16[30,96]{0,1:T(8,128)(2,1)S(1)}, u32[]{:S(2)}, u32[]{:S(2)}) collective-permute-start(bf16[30,96]{0,1:T(8,128)(2,1)S(1)} %slice.268), channel_id=1, source_target_pairs={{0,16},{16,32},{32,48},{48,64},{64,80},{80,96},{96,112},{112,128},... | collective-permute-start | bytes 17288 | tf_op jit(solution)/shard_map/ppermute | solution.py:21
  119.6 107.0 %all-gather.5.cloned.1.call-start = ((), (), s32[]{:S(2)}) async-start(), calls=%async_computation.8 | async-start | bytes 4456448 | tf_op jit(solution)/shard_map/all_gather | solution.py:155
  183.5 58.9 %all-reduce.6.cloned.1.call-start = ((), (), s32[]{:S(2)}) async-start(), calls=%async_computation.5 | async-start | bytes 1048576 | tf_op jit(solution)/shard_map/psum | solution.py:45
Sparse Core Ops, SparseCore 0:
  44.5 42.0 all-gather.2
  98.7 63.8 reduce-scatter.1
  183.6 42.9 all-gather.4
Sparse Core Ops, SparseCore 1:
  119.7 74.0 all-reduce.3
  196.5 39.0 all-reduce.5
where the time goes:
time: 252 us; the launch traced here: 251 us
  waiting for transfers between devices  128 us (51%)
  blocking collectives  56.2 us (22%)
  local copies, waits for them, and re-layouts  20.4 us (8%)
  between operations  15.5 us (6%)
  matrix products  13.9 us (6%)
  other arithmetic  13.6 us (5%)
  starting transfers between devices  3.48 us (1%)
    reduce_scatter x1, waiting for transfers between devices, local(): lax.psum_scatter(jnp.dot(hidden, down_w, preferred_element_type=jnp.float...  42.9 us
    all_gather x1, waiting for transfers between devices, local(): block_rows = lax.all_gather(arrived, TP, axis=0, tiled=True)  42.1 us
    all_gather x1, waiting for transfers between devices, local(): lax.all_gather(returned, TP, axis=0, tiled=True)  32.8 us
    all_to_all x1, blocking collectives, local(): lax.all_to_all(sending, 'ep', split_axis=1, concat_axis=1, tiled=True)  24.8 us
    all_to_all x1, blocking collectives, local(): lax.all_to_all(summed.reshape(slot_share, experts, width), 'ep', split_ax...  18.9 us
    all_to_all x1, blocking collectives, sent_to_all(): return lax.all_to_all(copies, axis, split_axis=0, concat_axis=0, tiled=True)  12.5 us
    psum x2, waiting for transfers between devices, by_axis(): x = lax.psum(x, axis)  9.51 us
    gather x2, local copies, waits for them, and re-layouts, local(): picked = jnp.take(every_slot, slot_index * experts + flat_ids, axis=0)  9.37 us
  transfers between devices with their start and end apart: 6, of which 5 were waited for; matrix products, arithmetic and copies ran while one was open for 9% of the time, Pallas kernels for 0%

commit v1 on v0

v1 whole, which is shorter than its diff:
```python
import jax
import jax.numpy as jnp
from jax import lax
from jax.sharding import Mesh
from jax.sharding import PartitionSpec as P

CONV_CH = 1536
CONV_W = 31
TOP_K = 4
TP = ("yh", "yl", "c")
GROUP = 4


epsilon = 1e-05
clamp_limit = 7.0
swish_slope = 1.702


def shifted(block, axis, distance):
    devices = range(lax.axis_size(axis))
    route = [(i - distance, i) for i in devices if i - distance in devices]
    return lax.ppermute(block, axis, route)


def swapped(x, axis):
    return lax.ppermute(x, axis, [(0, 1), (1, 0)])


def exchanged(x, axis):
    return lax.all_to_all(x, axis, split_axis=0, concat_axis=0, tiled=True)


def sent_to_all(x, axis):
    copies = jnp.broadcast_to(x, (lax.axis_size(axis), *x.shape))
    return exchanged(copies, axis)


def total_over(x, axis):
    size = lax.axis_size(axis)
    parts = exchanged(x.reshape(size, x.shape[0] // size, x.shape[1]), axis)
    share = jnp.sum(parts.astype(jnp.float32), axis=0).astype(jnp.bfloat16)
    return lax.all_gather(share, axis, axis=0, tiled=True)


def row_norm(inputs, gains):
    widened = inputs.astype(jnp.float32)
    row_mean = jnp.mean(widened, axis=-1, keepdims=True)
    row_var = jnp.mean(jnp.square(widened - row_mean), axis=-1, keepdims=True)
    return (widened - row_mean) * lax.rsqrt(row_var + epsilon) * gains


def mixer_part(mixer_in, mixer_gain, w_value, w_gate, w_taps, channel_gain, w_output):
    normed = row_norm(mixer_in, mixer_gain).astype(jnp.bfloat16)
    values = jnp.dot(normed, w_value, preferred_element_type=jnp.float32)
    gate_pre = jnp.dot(normed, w_gate, preferred_element_type=jnp.float32)
    gated_values = (values * jax.nn.sigmoid(gate_pre)).astype(jnp.bfloat16)
    mixer_rows = gated_values.shape[0]
    reach_rows = CONV_W - 1
    earlier = shifted(gated_values[mixer_rows - reach_rows :], "ep", 1)
    extended = jnp.concatenate([earlier, gated_values], axis=0)
    conv_out = jnp.zeros(gated_values.shape, jnp.float32)
    for offset in range(CONV_W):
        conv_out = (
            conv_out + extended[offset : offset + mixer_rows].astype(jnp.float32) * w_taps[offset]
        )
    sums = jnp.concatenate([jnp.sum(conv_out, axis=1), jnp.sum(conv_out * conv_out, axis=1)])
    sums = jnp.sum(sent_to_all(sums[None], TP), axis=(0, 1))
    row_mean = (sums[:mixer_rows] / CONV_CH)[:, None]
    row_var = (sums[mixer_rows:] / CONV_CH)[:, None] - row_mean * row_mean
    activated = jax.nn.silu(
        (conv_out - row_mean) * lax.rsqrt(row_var + epsilon) * channel_gain
    ).astype(jnp.bfloat16)
    return jnp.dot(activated, w_output, preferred_element_type=jnp.float32).astype(jnp.bfloat16)


def local(
    mixer_in,
    mixer_gain,
    w_value,
    w_gate,
    w_taps,
    channel_gain,
    w_output,
    expert_in,
    expert_gain,
    route_experts,
    route_scores,
    expert_gate,
    expert_up,
    expert_down,
):
    rows_b, width = expert_in.shape
    experts = lax.axis_size("ep")
    capacity = 2 * rows_b * TOP_K // experts
    slots = capacity // GROUP
    member = lax.axis_index(("yl", "c"))

    gate_up = jnp.concatenate([expert_gate[0], expert_up[0]], axis=1)
    down = expert_down[0]
    gu_y, down_y = swapped(gate_up, "yl"), swapped(down, "yl")
    gu_c, down_c = swapped(gate_up, "c"), swapped(down, "c")
    gu_d, down_d = swapped(gu_y, "c"), swapped(down_y, "c")

    normed_b = row_norm(expert_in, expert_gain).astype(jnp.bfloat16)
    ids = route_experts.T
    raised = jnp.exp(route_scores).T
    route_weights = raised / jnp.sum(raised, axis=0, keepdims=True)
    names = jnp.arange(experts, dtype=jnp.int32)[:, None]
    named = jnp.stack([ids[k][None, :] == names for k in range(TOP_K)])
    chosen = jnp.any(named, axis=0)
    weights = jnp.sum(jnp.where(named, route_weights[:, None, :], 0.0), axis=0)
    order = jnp.arange(rows_b, dtype=jnp.int32)
    before = (order[:, None] < order[None, :]).astype(jnp.bfloat16)
    rank = jnp.dot(chosen.astype(jnp.bfloat16), before, preferred_element_type=jnp.float32)
    place = jnp.where(chosen, rank.astype(jnp.int32), -1)
    own_slots = member + GROUP * jnp.arange(slots, dtype=jnp.int32)
    taken = place[:, None, :] == own_slots[None, :, None]
    select = taken.astype(jnp.bfloat16).reshape(experts * slots, rows_b)
    mixing = jnp.where(taken, weights[:, None, :], 0.0).reshape(experts * slots, rows_b)
    mixing_hi = mixing.astype(jnp.bfloat16)
    mixing_lo = (mixing - mixing_hi.astype(jnp.float32)).astype(jnp.bfloat16)

    sending = jnp.dot(select, normed_b, preferred_element_type=jnp.float32).astype(jnp.bfloat16)
    arrived = exchanged(sending.reshape(experts, slots, width), "ep").reshape(-1, width)

    mixer_partial = mixer_part(
        mixer_in, mixer_gain, w_value, w_gate, w_taps, channel_gain, w_output
    )
    mixer_out = total_over(mixer_partial, TP)

    hidden = []
    for gu in (gate_up, gu_c, gu_y, gu_d):
        both = jnp.dot(arrived, gu, preferred_element_type=jnp.float32)
        half = both.shape[1] // 2
        g = jnp.minimum(both[:, :half], clamp_limit)
        u = jnp.clip(both[:, half:], -clamp_limit, clamp_limit)
        hidden.append(((u + 1.0) * g * jax.nn.sigmoid(swish_slope * g)).astype(jnp.bfloat16))
    hidden = jnp.concatenate(hidden, axis=1)
    downs = jnp.concatenate([down, down_c, down_y, down_d], axis=0)
    partial = jnp.dot(hidden, downs, preferred_element_type=jnp.float32).astype(jnp.bfloat16)
    returned = exchanged(partial.reshape(experts, slots, width), "ep").reshape(-1, width)

    def mixed(m):
        return lax.dot_general(
            m, returned, (((0,), (0,)), ((), ())), preferred_element_type=jnp.float32
        )

    combined = (mixed(mixing_hi) + mixed(mixing_lo)).astype(jnp.bfloat16)
    expert_out = total_over(combined, TP)
    return (mixer_out, expert_out)


def solution(mesh):
    split = Mesh(mesh.devices.reshape(mesh.shape["ep"], 4, 2, 2), ("ep", *TP))
    in_specs = (
        P("ep", None),
        P(),
        P(None, TP),
        P(None, TP),
        P(None, TP),
        P(TP),
        P(TP, None),
        P("ep", None),
        P(),
        P("ep", None),
        P("ep", None),
        P("ep", None, TP),
        P("ep", None, TP),
        P("ep", TP, None),
    )
    out_specs = (P("ep", None), P("ep", None))
    return jax.shard_map(local, mesh=split, in_specs=in_specs, out_specs=out_specs, check_vma=False)
```

time: 252 us -> 192 us (0.76)
  waiting for transfers between devices: 128 us -> 59.6 us
  starting transfers between devices: 3.48 us -> 62.8 us
  local copies, waits for them, and re-layouts: 20.4 us -> 4.85 us
  between operations: 15.5 us -> 1.23 us
  blocking collectives: 56.2 us -> 42.7 us
  other arithmetic: 13.6 us -> 6.34 us
    all_gather x2 -> x0, waiting for transfers between devices: 74.9 us -> none  [the longest x1 42.1 us: local(): block_rows = lax.all_gather(arrived, TP, axis=0, tiled=True)]
    all_to_all x3 -> x0, blocking collectives: 56.2 us -> none  [the longest x1 24.8 us: local(): lax.all_to_all(sending, 'ep', split_axis=1, concat_axis=1, tiled=True)]
    all_to_all x0 -> x5, starting transfers between devices: none -> 43 us  [exchanged(): return lax.all_to_all(x, axis, split_axis=0, concat_axis=0, tiled=True)]
    reduce_scatter x1 -> x0, waiting for transfers between devices: 42.9 us -> none  [local(): lax.psum_scatter(jnp.dot(hidden, down_w, preferred_element_type=jnp.float...]
    all_gather x0 -> x2, blocking collectives: none -> 42.7 us  [total_over(): return lax.all_gather(share, axis, axis=0, tiled=True)]
    all_to_all x0 -> x5, waiting for transfers between devices: none -> 40.5 us  [exchanged(): return lax.all_to_all(x, axis, split_axis=0, concat_axis=0, tiled=True)]
    ppermute x0 -> x6, waiting for transfers between devices: none -> 18.3 us  [swapped(): return lax.ppermute(x, axis, [(0, 1), (1, 0)])]
    ppermute x0 -> x6, starting transfers between devices: none -> 16.4 us  [swapped(): return lax.ppermute(x, axis, [(0, 1), (1, 0)])]
  transfers between devices with their start and end apart: 6 -> 12, of which waited for: 5 -> 4; matrix products, arithmetic and copies ran while one was open for 9% -> 9% of each run, Pallas kernels for 0% -> 0%
where the time goes in v1:
time: 192 us; the launch traced here: 191 us
  starting transfers between devices  62.8 us (33%)
  waiting for transfers between devices  59.6 us (31%)
  blocking collectives  42.7 us (22%)
  matrix products  13.2 us (7%)
  other arithmetic  6.34 us (3%)
  local copies, waits for them, and re-layouts  4.85 us (3%)
    all_to_all x5, starting transfers between devices, exchanged(): return lax.all_to_all(x, axis, split_axis=0, concat_axis=0, tiled=True)  43 us
    all_gather x2, blocking collectives, total_over(): return lax.all_gather(share, axis, axis=0, tiled=True)  42.7 us
    all_to_all x5, waiting for transfers between devices, exchanged(): return lax.all_to_all(x, axis, split_axis=0, concat_axis=0, tiled=True)  40.5 us
    ppermute x6, waiting for transfers between devices, swapped(): return lax.ppermute(x, axis, [(0, 1), (1, 0)])  18.3 us
    ppermute x6, starting transfers between devices, swapped(): return lax.ppermute(x, axis, [(0, 1), (1, 0)])  16.4 us
    dot_general x4, matrix products, local(): both = jnp.dot(arrived, gu, preferred_element_type=jnp.float32)  4.64 us
  transfers between devices with their start and end apart: 12, of which 4 were waited for; matrix products, arithmetic and copies ran while one was open for 9% of the time, Pallas kernels for 0%

profile of v1, /device:TPU:1, one launch (start us, length us, event | category | flops | bytes accessed | tf_op | source)
XLA Modules:
  0.0 190.8 jit_solution(18122230676616447125)
XLA Ops:
  0.7 0.8 slice_bitcast_fusion.3
  1.6 0.6 copy-done.11
  2.1 0.1 eq.164
  2.2 1.2 convert_reduce_fusion
  3.4 1.3 fusion.23
  4.8 0.1 fusion.22
  4.9 1.5 fusion
  6.5 13.8 %all-to-all-start.2 = ((bf16[32,8,2048]{2,1,0:T(8,128)(2,1)}), bf16[32,8,2048]{2,1,0:T(8,128)(2,1)S(1)}, u32[]{:S(2)}, u32[]{:S(2)}) async-start(bf16[32,8,2048]{2,1,0:T(8,128)(2,1)} %fusion), calls=%async_computation.2 | async-start | bytes 2097152 | tf_op jit(solution)/shard_map/all_to_all | solution.py:30
  20.4 0.1 pad_maximum_fusion
  20.5 3.3 %collective-permute-start.2 = (bf16[2048,256]{1,0:T(8,128)(2,1)S(1)}, bf16[2048,256]{1,0:T(8,128)(2,1)S(1)}, u32[]{:S(2)}, u32[]{:S(2)}) collective-permute-start(bf16[2048,256]{1,0:T(8,128)(2,1)S(1)} %pad_maximum_fusion), channel_id=1, source_target_pairs={{0,2},{2,0},{1,3},{3,1},{4,6},{6,4},{5,7},{7,5},{8,10},{10,8},{9,1... | collective-permute-start | bytes 3145736 | tf_op jit(solution)/shard_map/ppermute | solution.py:26
  23.9 3.1 %collective-permute-start.1 = (bf16[2048,256]{1,0:T(8,128)(2,1)S(1)}, bf16[2048,256]{1,0:T(8,128)(2,1)}, u32[]{:S(2)}, u32[]{:S(2)}) collective-permute-start(bf16[2048,256]{1,0:T(8,128)(2,1)S(1)} %pad_maximum_fusion), channel_id=1, source_target_pairs={{0,1},{1,0},{2,3},{3,2},{4,5},{5,4},{6,7},{7,6},{8,9},{9,8},{10,11... | collective-permute-start | bytes 3145736 | tf_op jit(solution)/shard_map/ppermute | solution.py:26
  27.0 2.1 %collective-permute-start.5 = (bf16[128,2048]{1,0:T(8,128)(2,1)}, bf16[128,2048]{1,0:T(8,128)(2,1)}, u32[]{:S(2)}, u32[]{:S(2)}) collective-permute-start(bf16[128,2048]{1,0:T(8,128)(2,1)} %bitcast.43), channel_id=1, source_target_pairs={{0,2},{2,0},{1,3},{3,1},{4,6},{6,4},{5,7},{7,5},{8,10},{10,8},{9,1... | collective-permute-start | bytes 1572872 | tf_op jit(solution)/shard_map/ppermute | solution.py:26
  29.1 2.2 %collective-permute-start.4 = (bf16[128,2048]{1,0:T(8,128)(2,1)}, bf16[128,2048]{1,0:T(8,128)(2,1)}, u32[]{:S(2)}, u32[]{:S(2)}) collective-permute-start(bf16[128,2048]{1,0:T(8,128)(2,1)} %bitcast.43), channel_id=1, source_target_pairs={{0,1},{1,0},{2,3},{3,2},{4,5},{5,4},{6,7},{7,6},{8,9},{9,8},{10,11... | collective-permute-start | bytes 1572872 | tf_op jit(solution)/shard_map/ppermute | solution.py:26
  31.3 0.2 convert_reduce_fusion.1
  31.5 0.3 fusion.26
  31.8 0.4 fusion.122
  32.2 0.3 copy-done.23
  32.5 0.4 fusion.21
  32.9 0.1 slice.316
  33.0 3.4 %collective-permute-start = (bf16[30,96]{0,1:T(8,128)(2,1)S(1)}, bf16[30,96]{0,1:T(8,128)(2,1)S(1)}, u32[]{:S(2)}, u32[]{:S(2)}) collective-permute-start(bf16[30,96]{0,1:T(8,128)(2,1)S(1)} %slice.316), channel_id=1, source_target_pairs={{0,16},{16,32},{32,48},{48,64},{64,80},{80,96},{96,112},{112,128},... | collective-permute-start | bytes 17288 | tf_op jit(solution)/shard_map/ppermute | solution.py:22
  36.5 0.9 collective-permute-done
  37.3 1.5 fusion.124
  38.8 0.6 pad_maximum_fusion.2
  39.4 18.3 %collective-permute-done.5 = bf16[128,2048]{1,0:T(8,128)(2,1)} collective-permute-done((bf16[128,2048]{1,0:T(8,128)(2,1)}, bf16[128,2048]{1,0:T(8,128)(2,1)}, u32[]{:S(2)}, u32[]{:S(2)}) %collective-permute-start.5) | collective-permute-done | bytes 524320 | tf_op jit(solution)/shard_map/ppermute | solution.py:26
  57.7 3.7 %collective-permute-start.6 = (bf16[128,2048]{1,0:T(8,128)(2,1)}, bf16[128,2048]{1,0:T(8,128)(2,1)}, u32[]{:S(2)}, u32[]{:S(2)}) collective-permute-start(bf16[128,2048]{1,0:T(8,128)(2,1)} %collective-permute-done.5), channel_id=1, source_target_pairs={{0,1},{1,0},{2,3},{3,2},{4,5},{5,4},{6,7},{7,6},{8,9},{9,8},{10,11... | collective-permute-start | bytes 1572872 | tf_op jit(solution)/shard_map/ppermute | solution.py:26
  61.4 1.9 %collective-permute-start.3 = (bf16[2048,256]{1,0:T(8,128)(2,1)S(1)}, bf16[2048,256]{1,0:T(8,128)(2,1)}, u32[]{:S(2)}, u32[]{:S(2)}) collective-permute-start(bf16[2048,256]{1,0:T(8,128)(2,1)S(1)} %collective-permute-done.2), channel_id=1, source_target_pairs={{0,1},{1,0},{2,3},{3,2},{4,5},{5,4},{6,7},{7,6},{8,9},{9,8},{10,11... | collective-permute-start | bytes 3145736 | tf_op jit(solution)/shard_map/ppermute | solution.py:26
  63.3 1.3 broadcast_in_dim.30
  64.6 7.6 %all-to-all-start = ((f32[16,1,256]{2,1,0:T(1,128)}), f32[16,1,256]{2,1,0:T(1,128)}, u32[]{:S(2)}, u32[]{:S(2)}) async-start(f32[16,1,256]{2,1,0:T(1,128)} %broadcast_in_dim.30), calls=%async_computation | async-start | bytes 32768 | tf_op jit(solution)/shard_map/all_to_all | solution.py:30
  72.2 0.5 fusion.31
  72.8 1.8 fusion.33
  74.8 0.5 fusion.35
  75.4 1.7 fusion.29
  77.2 3.2 %fusion.1 = bf16[32,8,2048]{2,1,0:T(8,128)(2,1)} fusion(bf16[128,2048]{1,0:T(8,128)(2,1)} %collective-permute-done.6, bf16[128,2048]{1,0:T(8,128)(2,1)} %collective-permute-done.5, bf16[128,2048]{1,0:T(8,128)(2,1)} %collective-permute-done.4, bf16[128,2048]{1,0:T(8,128)(2,1)} %bitcast.43, bf16[256,128]{0,1:T(8,128)(2,1)S(1)} %fusion.52, ...), kind=kOutput, calls=%fused_computation.3 | convolution fusion | flops 546832384 | bytes 3407872 | tf_op jit(solution)/shard_map/dot_general | solution.py:140
  80.5 9.4 %all-to-all-start.3 = ((bf16[32,8,2048]{2,1,0:T(8,128)(2,1)}), bf16[32,8,2048]{2,1,0:T(8,128)(2,1)S(1)}, u32[]{:S(2)}, u32[]{:S(2)}) async-start(bf16[32,8,2048]{2,1,0:T(8,128)(2,1)} %fusion.1), calls=%async_computation.3 | async-start | bytes 2097152 | tf_op jit(solution)/shard_map/all_to_all | solution.py:30
  89.9 0.8 reduce_sum.109
  90.7 1.2 fusion.4
  91.9 25.0 %all-to-all-done.3 = bf16[32,8,2048]{2,1,0:T(8,128)(2,1)S(1)} async-done(((bf16[32,8,2048]{2,1,0:T(8,128)(2,1)}), bf16[32,8,2048]{2,1,0:T(8,128)(2,1)S(1)}, u32[]{:S(2)}, u32[]{:S(2)}) %all-to-all-start.3) | async-done | bytes 1048608 | tf_op jit(solution)/shard_map/all_to_all | solution.py:30
  116.9 8.7 %all-to-all-start.1 = ((bf16[16,8,2048]{2,1,0:T(8,128)(2,1)}), bf16[16,8,2048]{2,1,0:T(8,128)(2,1)S(1)}, u32[]{:S(2)}, u32[]{:S(2)}) async-start(bf16[16,8,2048]{2,1,0:T(8,128)(2,1)} %fusion.4), calls=%async_computation.1 | async-start | bytes 1048576 | tf_op jit(solution)/shard_map/all_to_all | solution.py:30
  125.8 0.4 convolution_bitcast_fusion
  126.2 1.2 fusion.5
  127.4 15.4 %all-to-all-done.1 = bf16[16,8,2048]{2,1,0:T(8,128)(2,1)S(1)} async-done(((bf16[16,8,2048]{2,1,0:T(8,128)(2,1)}), bf16[16,8,2048]{2,1,0:T(8,128)(2,1)S(1)}, u32[]{:S(2)}, u32[]{:S(2)}) %all-to-all-start.1) | async-done | bytes 524320 | tf_op jit(solution)/shard_map/all_to_all | solution.py:30
  142.9 3.5 %all-to-all-start.4 = ((bf16[16,8,2048]{2,1,0:T(8,128)(2,1)}), bf16[16,8,2048]{2,1,0:T(8,128)(2,1)S(1)}, u32[]{:S(2)}, u32[]{:S(2)}) async-start(bf16[16,8,2048]{2,1,0:T(8,128)(2,1)} %fusion.5), calls=%async_computation.4 | async-start | bytes 1048576 | tf_op jit(solution)/shard_map/all_to_all | solution.py:30
  146.3 0.1 reduce_sum.110
  146.4 26.8 %all_gather.6 = bf16[128,2048]{1,0:T(8,128)(2,1)S(1)} all-gather(bf16[8,2048]{1,0:T(8,128)(2,1)S(1)} %reduce_sum.110), channel_id=1, replica_groups=mesh['ep'=32,'yh'=4,'yl'=2,'c'=2] {'yh','yl','c'}, dimensions={0}, use_global_device_ids=true | all-gather | bytes 557056 | tf_op jit(solution)/shard_map/all_gather | solution.py:42
  173.2 0.1 reduce_sum.115
  173.3 15.9 %all_gather.7 = bf16[128,2048]{1,0:T(8,128)(2,1)S(1)} all-gather(bf16[8,2048]{1,0:T(8,128)(2,1)S(1)} %reduce_sum.115), channel_id=1, replica_groups=mesh['ep'=32,'yh'=4,'yl'=2,'c'=2] {'yh','yl','c'}, dimensions={0}, use_global_device_ids=true | all-gather | bytes 557056 | tf_op jit(solution)/shard_map/all_gather | solution.py:42
  189.2 0.8 copy.26
  190.0 0.8 copy.27
  (74 shorter events, 0.5 us)
Async XLA Ops:
  0.6 90.0 %copy-start = (bf16[96,2048]{1,0:T(8,128)(2,1)S(1)}, bf16[96,2048]{1,0:T(8,128)(2,1)}, u32[]{:S(2)}) copy-start(bf16[96,2048]{1,0:T(8,128)(2,1)} %param.20) | copy-start | bytes 1179652
  0.6 4.3 %copy-start.1 = (bf16[128,2048]{1,0:T(8,128)(2,1)S(1)}, bf16[128,2048]{1,0:T(8,128)(2,1)}, u32[]{:S(2)}) copy-start(bf16[128,2048]{1,0:T(8,128)(2,1)} %param.21) | copy-start | bytes 1572868
  0.7 4.3 %copy-start.9 = (f32[2048]{0:T(1024)S(1)}, f32[2048]{0:T(1024)}, u32[]{:S(2)}) copy-start(f32[2048]{0:T(1024)} %param.22) | copy-start | bytes 24580
  1.5 5.0 %copy-start.13 = (s32[128]{0:T(128)}, s32[128]{0:T(128)S(1)}, u32[]{:S(2)}) copy-start(s32[128]{0:T(128)S(1)} %get-tuple-element.36) | copy-start | bytes 1540
  1.5 5.0 %copy-start.15 = (s32[128]{0:T(128)}, s32[128]{0:T(128)S(1)}, u32[]{:S(2)}) copy-start(s32[128]{0:T(128)S(1)} %get-tuple-element.39) | copy-start | bytes 1540
  1.5 5.0 %copy-start.17 = (s32[128]{0:T(128)}, s32[128]{0:T(128)S(1)}, u32[]{:S(2)}) copy-start(s32[128]{0:T(128)S(1)} %get-tuple-element.37) | copy-start | bytes 1540
  1.5 4.9 %copy-start.19 = (s32[128]{0:T(128)}, s32[128]{0:T(128)S(1)}, u32[]{:S(2)}) copy-start(s32[128]{0:T(128)S(1)} %get-tuple-element.38) | copy-start | bytes 1540
  1.6 0.6 copy-start.11
  6.5 13.9 %copy-start.3 = (bf16[1,2048,128]{2,1,0:T(8,128)(2,1)S(1)}, bf16[1,2048,128]{2,1,0:T(8,128)(2,1)}, u32[]{:S(2)}) copy-start(bf16[1,2048,128]{2,1,0:T(8,128)(2,1)} %param.26) | copy-start | bytes 1572868
  6.5 13.9 %copy-start.5 = (bf16[1,2048,128]{2,1,0:T(8,128)(2,1)S(1)}, bf16[1,2048,128]{2,1,0:T(8,128)(2,1)}, u32[]{:S(2)}) copy-start(bf16[1,2048,128]{2,1,0:T(8,128)(2,1)} %param.25) | copy-start | bytes 1572868
  6.5 56.8 %all-to-all-start.2 = ((bf16[32,8,2048]{2,1,0:T(8,128)(2,1)}), bf16[32,8,2048]{2,1,0:T(8,128)(2,1)S(1)}, u32[]{:S(2)}, u32[]{:S(2)}) async-start(bf16[32,8,2048]{2,1,0:T(8,128)(2,1)} %fusion), calls=%async_computation.2 | async-start | bytes 2097152 | tf_op jit(solution)/shard_map/all_to_all | solution.py:30
  20.4 11.0 %copy-start.2 = (bf16[128,2048]{1,0:T(8,128)(2,1)S(1)}, bf16[128,2048]{1,0:T(8,128)(2,1)}, u32[]{:S(2)}) copy-start(bf16[128,2048]{1,0:T(8,128)(2,1)} %param.14) | copy-start | bytes 1572868
  20.5 11.3 %copy-start.22 = (bf16[2048,96]{0,1:T(8,128)(2,1)S(1)}, bf16[2048,96]{0,1:T(8,128)(2,1)}, u32[]{:S(2)}) copy-start(bf16[2048,96]{0,1:T(8,128)(2,1)} %param.16) | copy-start | bytes 1179652
  20.5 11.3 %copy-start.24 = (f32[2048]{0:T(1024)S(1)}, f32[2048]{0:T(1024)}, u32[]{:S(2)}) copy-start(f32[2048]{0:T(1024)} %param.15) | copy-start | bytes 24580
  20.5 40.8 %collective-permute-start.2 = (bf16[2048,256]{1,0:T(8,128)(2,1)S(1)}, bf16[2048,256]{1,0:T(8,128)(2,1)S(1)}, u32[]{:S(2)}, u32[]{:S(2)}) collective-permute-start(bf16[2048,256]{1,0:T(8,128)(2,1)S(1)} %pad_maximum_fusion), channel_id=1, source_target_pairs={{0,2},{2,0},{1,3},{3,1},{4,6},{6,4},{5,7},{7,5},{8,10},{10,8},{9,1... | collective-permute-start | bytes 3145736 | tf_op jit(solution)/shard_map/ppermute | solution.py:26
  23.9 49.0 %collective-permute-start.1 = (bf16[2048,256]{1,0:T(8,128)(2,1)S(1)}, bf16[2048,256]{1,0:T(8,128)(2,1)}, u32[]{:S(2)}, u32[]{:S(2)}) collective-permute-start(bf16[2048,256]{1,0:T(8,128)(2,1)S(1)} %pad_maximum_fusion), channel_id=1, source_target_pairs={{0,1},{1,0},{2,3},{3,2},{4,5},{5,4},{6,7},{7,6},{8,9},{9,8},{10,11... | collective-permute-start | bytes 3145736 | tf_op jit(solution)/shard_map/ppermute | solution.py:26
  27.0 30.6 %collective-permute-start.5 = (bf16[128,2048]{1,0:T(8,128)(2,1)}, bf16[128,2048]{1,0:T(8,128)(2,1)}, u32[]{:S(2)}, u32[]{:S(2)}) collective-permute-start(bf16[128,2048]{1,0:T(8,128)(2,1)} %bitcast.43), channel_id=1, source_target_pairs={{0,2},{2,0},{1,3},{3,1},{4,6},{6,4},{5,7},{7,5},{8,10},{10,8},{9,1... | collective-permute-start | bytes 1572872 | tf_op jit(solution)/shard_map/ppermute | solution.py:26
  29.1 48.1 %collective-permute-start.4 = (bf16[128,2048]{1,0:T(8,128)(2,1)}, bf16[128,2048]{1,0:T(8,128)(2,1)}, u32[]{:S(2)}, u32[]{:S(2)}) collective-permute-start(bf16[128,2048]{1,0:T(8,128)(2,1)} %bitcast.43), channel_id=1, source_target_pairs={{0,1},{1,0},{2,3},{3,2},{4,5},{5,4},{6,7},{7,6},{8,9},{9,8},{10,11... | collective-permute-start | bytes 1572872 | tf_op jit(solution)/shard_map/ppermute | solution.py:26
  31.5 1.0 copy-start.23
  32.5 3.9 %copy-start.8 = (f32[31,96]{1,0:T(8,128)S(1)}, f32[31,96]{1,0:T(8,128)}, u32[]{:S(2)}) copy-start(f32[31,96]{1,0:T(8,128)} %param.18) | copy-start | bytes 35716
  33.0 4.3 %collective-permute-start = (bf16[30,96]{0,1:T(8,128)(2,1)S(1)}, bf16[30,96]{0,1:T(8,128)(2,1)S(1)}, u32[]{:S(2)}, u32[]{:S(2)}) collective-permute-start(bf16[30,96]{0,1:T(8,128)(2,1)S(1)} %slice.316), channel_id=1, source_target_pairs={{0,16},{16,32},{32,48},{48,64},{64,80},{80,96},{96,112},{112,128},... | collective-permute-start | bytes 17288 | tf_op jit(solution)/shard_map/ppermute | solution.py:22
  57.7 19.5 %collective-permute-start.6 = (bf16[128,2048]{1,0:T(8,128)(2,1)}, bf16[128,2048]{1,0:T(8,128)(2,1)}, u32[]{:S(2)}, u32[]{:S(2)}) collective-permute-start(bf16[128,2048]{1,0:T(8,128)(2,1)} %collective-permute-done.5), channel_id=1, source_target_pairs={{0,1},{1,0},{2,3},{3,2},{4,5},{5,4},{6,7},{7,6},{8,9},{9,8},{10,11... | collective-permute-start | bytes 1572872 | tf_op jit(solution)/shard_map/ppermute | solution.py:26
  61.4 14.0 %collective-permute-start.3 = (bf16[2048,256]{1,0:T(8,128)(2,1)S(1)}, bf16[2048,256]{1,0:T(8,128)(2,1)}, u32[]{:S(2)}, u32[]{:S(2)}) collective-permute-start(bf16[2048,256]{1,0:T(8,128)(2,1)S(1)} %collective-permute-done.2), channel_id=1, source_target_pairs={{0,1},{1,0},{2,3},{3,2},{4,5},{5,4},{6,7},{7,6},{8,9},{9,8},{10,11... | collective-permute-start | bytes 3145736 | tf_op jit(solution)/shard_map/ppermute | solution.py:26
  64.6 15.9 %all-to-all-start = ((f32[16,1,256]{2,1,0:T(1,128)}), f32[16,1,256]{2,1,0:T(1,128)}, u32[]{:S(2)}, u32[]{:S(2)}) async-start(f32[16,1,256]{2,1,0:T(1,128)} %broadcast_in_dim.30), calls=%async_computation | async-start | bytes 32768 | tf_op jit(solution)/shard_map/all_to_all | solution.py:30
  72.8 1.9 %copy-start.4 = (bf16[1,2048,128]{2,1,0:T(8,128)(2,1)S(1)}, bf16[1,2048,128]{2,1,0:T(8,128)(2,1)}, u32[]{:S(2)}) copy-start(bf16[1,2048,128]{2,1,0:T(8,128)(2,1)} %param.26) | copy-start | bytes 1572868
  72.8 1.9 %copy-start.6 = (bf16[1,2048,128]{2,1,0:T(8,128)(2,1)S(1)}, bf16[1,2048,128]{2,1,0:T(8,128)(2,1)}, u32[]{:S(2)}) copy-start(bf16[1,2048,128]{2,1,0:T(8,128)(2,1)} %param.25) | copy-start | bytes 1572868
  80.4 9.4 %copy-start.10 = (f32[128,4]{0,1:T(4,128)S(1)}, f32[128,4]{0,1:T(4,128)}, u32[]{:S(2)}) copy-start(f32[128,4]{0,1:T(4,128)} %param.24) | copy-start | bytes 6148
  80.5 10.2 %copy-start.7 = (f32[128,96]{0,1:T(8,128)S(1)}, f32[128,96]{0,1:T(8,128)}, u32[]{:S(2)}) copy-start(f32[128,96]{0,1:T(8,128)} %get-tuple-element.4) | copy-start | bytes 147460
  80.5 10.2 %copy-start.21 = (f32[96]{0:T(128)S(1)}, f32[96]{0:T(128)}, u32[]{:S(2)}) copy-start(f32[96]{0:T(128)} %param.19) | copy-start | bytes 1156
  80.5 36.5 %all-to-all-start.3 = ((bf16[32,8,2048]{2,1,0:T(8,128)(2,1)}), bf16[32,8,2048]{2,1,0:T(8,128)(2,1)S(1)}, u32[]{:S(2)}, u32[]{:S(2)}) async-start(bf16[32,8,2048]{2,1,0:T(8,128)(2,1)} %fusion.1), calls=%async_computation.3 | async-start | bytes 2097152 | tf_op jit(solution)/shard_map/all_to_all | solution.py:30
  89.8 35.8 %copy-start.18 = (s32[128]{0:T(128)S(1)}, s32[128]{0:T(128)}, u32[]{:S(2)}) copy-start(s32[128]{0:T(128)} %copy-done.17) | copy-start | bytes 1540
  89.8 35.8 %copy-start.20 = (s32[128]{0:T(128)S(1)}, s32[128]{0:T(128)}, u32[]{:S(2)}) copy-start(s32[128]{0:T(128)} %copy-done.19) | copy-start | bytes 1540
  89.9 35.8 %copy-start.14 = (s32[128]{0:T(128)S(1)}, s32[128]{0:T(128)}, u32[]{:S(2)}) copy-start(s32[128]{0:T(128)} %copy-done.13) | copy-start | bytes 1540
  89.9 35.8 %copy-start.16 = (s32[128]{0:T(128)S(1)}, s32[128]{0:T(128)}, u32[]{:S(2)}) copy-start(s32[128]{0:T(128)} %copy-done.15) | copy-start | bytes 1540
  90.7 35.1 %copy-start.12 = (s32[8]{0:T(128)S(1)}, s32[8]{0:T(128)}, u32[]{:S(2)}) copy-start(s32[8]{0:T(128)} %copy-done.11) | copy-start | bytes 100
  116.9 25.9 %all-to-all-start.1 = ((bf16[16,8,2048]{2,1,0:T(8,128)(2,1)}), bf16[16,8,2048]{2,1,0:T(8,128)(2,1)S(1)}, u32[]{:S(2)}, u32[]{:S(2)}) async-start(bf16[16,8,2048]{2,1,0:T(8,128)(2,1)} %fusion.4), calls=%async_computation.1 | async-start | bytes 1048576 | tf_op jit(solution)/shard_map/all_to_all | solution.py:30
  142.9 30.3 %all-to-all-start.4 = ((bf16[16,8,2048]{2,1,0:T(8,128)(2,1)}), bf16[16,8,2048]{2,1,0:T(8,128)(2,1)S(1)}, u32[]{:S(2)}, u32[]{:S(2)}) async-start(bf16[16,8,2048]{2,1,0:T(8,128)(2,1)} %fusion.5), calls=%async_computation.4 | async-start | bytes 1048576 | tf_op jit(solution)/shard_map/all_to_all | solution.py:30
